TPU v7x, 32 devices: a whole 2x2x4 slice. The times are simulated.
32 devices in a mesh: ep: 8 (over z, core), tp: 4 (over y, x).
Axes of the slice: x: 2, y: 2, z: 4, core: 2. Of those that a mesh axis runs over, the one named last changes fastest.
Arguments:
- tokens: bfloat16 [128, 4096], P('ep', 'tp'), may hold values from -40 to 40
- norm_gain: bfloat16 [4096], P('tp'), may hold values from 0.099609375 to 1.8984375
- routes: int32 [128, 4], P('ep'), may hold values from 0 to 7, all different within a row; in each aligned block of 16 rows (0 to 15, 16 to 31, ...) at most 16 rows name the same one
- route_weights: float32 [128, 4], P('ep'), may hold values from 0.05 to 1
- w_gate: bfloat16 [8, 4096, 4096], P('ep', None, 'tp'), may hold values from -0.25 to 0.25
- w_up: bfloat16 [8, 4096, 4096], P('ep', None, 'tp'), may hold values from -0.25 to 0.25
- w_down: bfloat16 [8, 4096, 4096], P('ep', 'tp'), may hold values from -0.0234375 to 0.0234375
Outputs:
- mixed: bfloat16 [128, 4096], P('ep', 'tp')
Inputs may be any that keep to these rules, and one draw needn't show every extreme that they name: `routes`: within the 16 rows of one device, each token names 4 different experts, and no expert is named by more than 16 rows; some expert reaches 16.
All inputs are finite; a program needn't handle non-finite values.
Results may differ from a plain program's by a relative error of at most 0.018.
Values may be sent and summed in bfloat16 or wider, within the bound.
No kernel may reach another device: no remote copies, remote signals or barrier semaphores. Data moves between devices by JAX's collectives and lax.ppermute only.
A program may use at most 64 MiB of HBM per device.

v0:
```python
import jax
import jax.numpy as jnp
from jax import lax
from jax.sharding import PartitionSpec as P


def shards(tokens, norm_gain, routes, route_weights, w_gate, w_up, w_down):
    tok_rows = tokens.shape[0]
    topk = routes.shape[1]
    groups = lax.axis_size("ep")
    capacity = min(tok_rows, max(2, 2 * tok_rows * topk // groups))
    slot_rows = groups * capacity
    flat = routes.reshape(-1)
    order = jnp.arange(flat.shape[0], dtype=jnp.int32)
    earlier = (flat[:, None] == flat[None, :]) & (order[:, None] > order[None, :])
    slot = jnp.sum(earlier.astype(jnp.int32), axis=1)
    target = (flat * capacity + slot).reshape(tok_rows, topk)
    slot_ids = jnp.arange(slot_rows, dtype=jnp.int32)
    picker = jnp.any(target[None, :, :] == slot_ids[:, None, None], axis=2).astype(jnp.bfloat16)
    combine = jnp.sum(
        jnp.where(target[:, :, None] == slot_ids[None, None, :], route_weights[:, :, None], 0.0),
        axis=1,
    )
    whole, gain_whole = (
        lax.all_gather(tokens, "tp", axis=1, tiled=True),
        lax.all_gather(norm_gain.reshape(1, -1), "tp", axis=1, tiled=True),
    )
    full_values = whole.astype(jnp.float32)
    scale = lax.rsqrt(jnp.mean(full_values * full_values, axis=1, keepdims=True) + 1e-05)
    normed = (full_values * scale * gain_whole.astype(jnp.float32)).astype(jnp.bfloat16)
    outbound = jnp.dot(picker, normed, preferred_element_type=jnp.float32).astype(jnp.bfloat16)
    arrived = lax.all_to_all(
        outbound.reshape(groups, capacity, -1), "ep", split_axis=0, concat_axis=0, tiled=True
    ).reshape(slot_rows, -1)
    gate_pre = jnp.dot(arrived, w_gate[0], preferred_element_type=jnp.float32)
    up_pre = jnp.dot(arrived, w_up[0], preferred_element_type=jnp.float32)
    gated = jnp.minimum(gate_pre, 7.0)
    upper = jnp.clip(up_pre, -7.0, 7.0)
    hidden = ((upper + 1.0) * gated * jax.nn.sigmoid(1.702 * gated)).astype(jnp.bfloat16)
    partial_out = jnp.dot(hidden, w_down[0], preferred_element_type=jnp.float32).astype(
        jnp.bfloat16
    )
    summed = (
        lax.psum_scatter(partial_out, "tp", scatter_dimension=1, tiled=True)
        .astype(jnp.float32)
        .astype(jnp.bfloat16)
    )
    returned = lax.all_to_all(
        summed.reshape(groups, capacity, -1), "ep", split_axis=0, concat_axis=0, tiled=True
    ).reshape(slot_rows, -1)
    mixed = jnp.dot(combine, returned.astype(jnp.float32), precision=lax.Precision.HIGHEST)
    return mixed.astype(jnp.bfloat16)


def solution(mesh):
    placed = (
        P("ep", "tp"),
        P("tp"),
        P("ep", None),
        P("ep", None),
        P("ep", None, "tp"),
        P("ep", None, "tp"),
        P("ep", "tp", None),
    )
    return jax.shard_map(
        shards, mesh=mesh, in_specs=placed, out_specs=P("ep", "tp"), check_vma=False
    )
```

profile of v0, /device:TPU:0, one launch (start us, length us, event | category | flops | bytes accessed | tf_op | source)
XLA Modules:
  0.0 120.4 jit_solution(6978321878295605920)
XLA Ops:
  6.5 0.0 reduce-scatter.2.cloned.1.call-start
  6.5 10.1 %all_gather.6 = bf16[16,4096]{1,0:T(8,128)(2,1)S(1)} all-gather(bf16[16,1024]{1,0:T(8,128)(2,1)} %param.7), channel_id=1, replica_groups=mesh['ep'=8,'tp'=4] {'tp'}, dimensions={1}, use_global_device_ids=true | all-gather | bytes 163840 | tf_op jit(solution)/shard_map/all_gather | solution.py:25
  16.7 0.1 fusion.34
  16.8 0.8 copy.21
  17.6 0.1 eq.20
  17.7 0.2 convert_reduce_fusion
  17.9 0.1 reduce_sum.30
  17.9 0.1 copy.22
  18.0 0.7 multiply_add_fusion
  18.7 0.1 fusion.45
  18.8 7.9 %all-gather = bf16[4096]{0:T(1024)(128)(2,1)S(1)} all-gather(bf16[1024]{0:T(1024)(128)(2,1)} %param.8), channel_id=2, replica_groups=mesh['ep'=8,'tp'=4] {'tp'}, dimensions={0}, use_global_device_ids=true | all-gather | bytes 10240 | tf_op jit(solution)/shard_map/all_gather | solution.py:26
  26.7 0.5 convolution_convert_fusion
  27.2 31.2 %all_to_all.10 = bf16[8,16,4096]{2,1,0:T(8,128)(2,1)S(1)} all-to-all(bf16[8,16,4096]{2,1,0:T(8,128)(2,1)S(1)} %bitcast.36), channel_id=1, replica_groups=mesh['ep'=8,'tp'=4] {'ep'}, dimensions={0} | all-to-all | bytes 2097152 | tf_op jit(solution)/shard_map/all_to_all | solution.py:32
  58.4 4.6 %fusion.9 = f32[128,1024]{1,0:T(8,128)S(1)} fusion(bf16[128,4096]{1,0:T(8,128)(2,1)S(1)} %bitcast.34, bf16[1,4096,1024]{2,1,0:T(8,128)(2,1)} %param.11), kind=kOutput, calls=%fused_computation.8 | convolution fusion | flops 1073872896 | bytes 9961472 | tf_op jit(solution)/shard_map/dot_general | solution.py:35
  63.1 0.0 copy-start
  63.1 9.3 %fusion.6 = bf16[128,4096]{1,0:T(8,128)(2,1)} fusion(bf16[1,1024,4096]{2,1,0:T(8,128)(2,1)} %param.13, f32[128,1024]{1,0:T(8,128)S(1)} %fusion.9, bf16[128,4096]{1,0:T(8,128)(2,1)S(1)} %bitcast.35, bf16[1,4096,1024]{2,1,0:T(8,128)(2,1)} %param.12), kind=kOutput, calls=%fused_computation.6 | convolution fusion | flops 2149187584 | bytes 19398656 | tf_op jit(solution)/shard_map/dot_general | solution.py:40
  72.4 0.0 reduce-scatter.2.cloned.1.call-update
  72.4 26.0 %reduce-scatter.2.cloned.1.call-done = bf16[128,1024]{1,0:T(8,128)(2,1)} async-done(((bf16[128,4096]{1,0:T(8,128)(2,1)}), bf16[128,1024]{1,0:T(8,128)(2,1)}) %reduce-scatter.2.cloned.1.call-update) | async-done | bytes 262160 | tf_op jit(solution)/shard_map/reduce_scatter | solution.py:44
  98.4 4.6 %all-to-all-start.1 = ((bf16[8,16,1024]{2,1,0:T(8,128)(2,1)}), bf16[8,16,1024]{2,1,0:T(8,128)(2,1)S(1)}, u32[]{:S(2)}, u32[]{:S(2)}) async-start(bf16[8,16,1024]{2,1,0:T(8,128)(2,1)} %bitcast.38), calls=%async_computation.2 | async-start | bytes 524288 | tf_op jit(solution)/shard_map/all_to_all | solution.py:48
  103.0 0.0 copy-done
  103.1 0.1 select_reduce_fusion
  103.1 9.6 %all-to-all-done.1 = bf16[8,16,1024]{2,1,0:T(8,128)(2,1)S(1)} async-done(((bf16[8,16,1024]{2,1,0:T(8,128)(2,1)}), bf16[8,16,1024]{2,1,0:T(8,128)(2,1)S(1)}, u32[]{:S(2)}, u32[]{:S(2)}) %all-to-all-start.1) | async-done | bytes 262176 | tf_op jit(solution)/shard_map/all_to_all | solution.py:48
  112.8 0.8 convolution_convert_fusion.1
  (2 shorter events, 0.0 us)
Async XLA Ops:
  6.5 91.9 %reduce-scatter.2.cloned.1.call-start = ((), (), s32[]{:S(2)}) async-start(), calls=%async_computation.3 | async-start | bytes 1310720 | tf_op jit(solution)/shard_map/reduce_scatter | solution.py:44
  63.1 40.0 %copy-start = (f32[16,4]{0,1:T(4,128)S(1)}, f32[16,4]{0,1:T(4,128)}, u32[]{:S(2)}) copy-start(f32[16,4]{0,1:T(4,128)} %param.10) | copy-start | bytes 772
  98.4 14.3 %all-to-all-start.1 = ((bf16[8,16,1024]{2,1,0:T(8,128)(2,1)}), bf16[8,16,1024]{2,1,0:T(8,128)(2,1)S(1)}, u32[]{:S(2)}, u32[]{:S(2)}) async-start(bf16[8,16,1024]{2,1,0:T(8,128)(2,1)} %bitcast.38), calls=%async_computation.2 | async-start | bytes 524288 | tf_op jit(solution)/shard_map/all_to_all | solution.py:48
Sparse Core Ops, SparseCore 0:
  72.5 25.8 reduce-scatter.1
where the time goes:
time: 121 us; the launch traced here: 120 us
  blocking collectives  49.2 us (41%)
  waiting for transfers between devices  35.7 us (30%)
  matrix products  15.2 us (13%)
  between operations  13.4 us (11%)
  starting transfers between devices  4.62 us (4%)
    all_to_all x1, blocking collectives, shards(): lax.all_to_all(outbound.reshape(groups, capacity, -1), 'ep', split_axis=0...  31.2 us
    reduce_scatter x1, waiting for transfers between devices, shards(): lax.psum_scatter(partial_out, 'tp', scatter_dimension=1, tiled=True)  26 us
    all_gather x1, blocking collectives, shards(): lax.all_gather(tokens, 'tp', axis=1, tiled=True)  10.1 us
    all_to_all x1, waiting for transfers between devices, shards(): lax.all_to_all(summed.reshape(groups, capacity, -1), 'ep', split_axis=0,...  9.62 us
    dot_general x1, matrix products, shards(): jnp.dot(hidden, w_down[0], preferred_element_type=jnp.float32)  9.29 us
    all_gather x1, blocking collectives, shards(): lax.all_gather(norm_gain.reshape(1, -1), 'tp', axis=1, tiled=True)  7.86 us
    dot_general x1, matrix products, shards(): gate_pre = jnp.dot(arrived, w_gate[0], preferred_element_type=jnp.float32)  4.63 us
    all_to_all x1, starting transfers between devices, shards(): lax.all_to_all(summed.reshape(groups, capacity, -1), 'ep', split_axis=0,...  4.61 us
  transfers between devices with their start and end apart: 2, of which 2 were waited for; matrix products, arithmetic and copies ran while one was open for 0% of the time, Pallas kernels for 0%

commit v1 on v0

--- a/solution.py
+++ b/solution.py
@@ -2,6 +2,7 @@
 import jax.numpy as jnp
 from jax import lax
 from jax.sharding import PartitionSpec as P
+from jax.lax import all_gather
 
 
 def shards(tokens, norm_gain, routes, route_weights, w_gate, w_up, w_down):
@@ -22,7 +23,7 @@
         axis=1,
     )
     whole, gain_whole = (
-        lax.all_gather(tokens, "tp", axis=1, tiled=True),
+        jnp.concatenate(all_gather(tokens, "tp"), axis=1),
         lax.all_gather(norm_gain.reshape(1, -1), "tp", axis=1, tiled=True),
     )
     full_values = whole.astype(jnp.float32)

time: 121 us -> 121 us (level)
  no operation moved by 1% of the time
where the time goes in v1:
time: 121 us
  blocking collectives  49.2 us (41%)
  waiting for transfers between devices  35.6 us (29%)
  matrix products  15.2 us (13%)
  between operations  13.5 us (11%)
  starting transfers between devices  4.61 us (4%)
  local copies, waits for them, and re-layouts  1.36 us (1%)
  other arithmetic  1.21 us (1%)
    all_to_all x1, blocking collectives, shards(): lax.all_to_all(outbound.reshape(groups, capacity, -1), 'ep', split_axis=0...  31.2 us
    reduce_scatter x1, waiting for transfers between devices, shards(): lax.psum_scatter(partial_out, 'tp', scatter_dimension=1, tiled=True)  26 us
    all_gather x1, blocking collectives, shards(): all_gather(tokens, 'tp')  10.1 us
    all_to_all x1, waiting for transfers between devices, shards(): lax.all_to_all(summed.reshape(groups, capacity, -1), 'ep', split_axis=0,...  9.62 us
    dot_general x1, matrix products, shards(): jnp.dot(hidden, w_down[0], preferred_element_type=jnp.float32)  9.29 us
    all_gather x1, blocking collectives, shards(): lax.all_gather(norm_gain.reshape(1, -1), 'tp', axis=1, tiled=True)  7.86 us
    dot_general x1, matrix products, shards(): gate_pre = jnp.dot(arrived, w_gate[0], preferred_element_type=jnp.float32)  4.63 us
    all_to_all x1, starting transfers between devices, shards(): lax.all_to_all(summed.reshape(groups, capacity, -1), 'ep', split_axis=0,...  4.61 us
  transfers between devices with their start and end apart: 2, of which 2 were waited for; matrix products, arithmetic and copies ran while one was open for 0% of the time, Pallas kernels for 0%

profile of v1, /device:TPU:0, one launch (start us, length us, event | category | flops | bytes accessed | tf_op | source)
XLA Modules:
  0.0 120.8 jit_solution(14975321849657156243)
XLA Ops:
  6.5 0.0 reduce-scatter.2.cloned.1.call-start
  6.5 10.1 %all-gather = bf16[64,1024]{1,0:T(8,128)(2,1)S(1)} all-gather(bf16[16,1024]{1,0:T(8,128)(2,1)} %param.7), channel_id=2, replica_groups=mesh['ep'=8,'tp'=4] {'tp'}, dimensions={0}, use_global_device_ids=true | all-gather | bytes 163840 | tf_op jit(solution)/shard_map/all_gather | solution.py:26
  16.7 0.2 copy.26
  16.9 0.2 copy.27
  17.0 0.1 multiply_reduce_fusion
  17.2 0.8 copy.24
  18.0 0.1 eq.20
  18.0 0.2 convert_reduce_fusion
  18.2 0.1 reduce_sum.30
  18.3 0.1 copy.25
  18.4 0.7 multiply_add_fusion
  19.1 0.1 fusion.41
  19.2 7.9 %all-gather.1 = bf16[4096]{0:T(1024)(128)(2,1)S(1)} all-gather(bf16[1024]{0:T(1024)(128)(2,1)} %param.8), channel_id=3, replica_groups=mesh['ep'=8,'tp'=4] {'tp'}, dimensions={0}, use_global_device_ids=true | all-gather | bytes 10240 | tf_op jit(solution)/shard_map/all_gather | solution.py:27
  27.1 0.5 convolution_convert_fusion
  27.5 31.2 %all_to_all.10 = bf16[8,16,4096]{2,1,0:T(8,128)(2,1)S(1)} all-to-all(bf16[8,16,4096]{2,1,0:T(8,128)(2,1)S(1)} %bitcast.42), channel_id=1, replica_groups=mesh['ep'=8,'tp'=4] {'ep'}, dimensions={0} | all-to-all | bytes 2097152 | tf_op jit(solution)/shard_map/all_to_all | solution.py:33
  58.8 4.6 %fusion.9 = f32[128,1024]{1,0:T(8,128)S(1)} fusion(bf16[128,4096]{1,0:T(8,128)(2,1)S(1)} %bitcast.40, bf16[1,4096,1024]{2,1,0:T(8,128)(2,1)} %param.11), kind=kOutput, calls=%fused_computation.8 | convolution fusion | flops 1073872896 | bytes 9961472 | tf_op jit(solution)/shard_map/dot_general | solution.py:36
  63.4 0.0 copy-start
  63.4 9.3 %fusion.6 = bf16[128,4096]{1,0:T(8,128)(2,1)} fusion(bf16[1,1024,4096]{2,1,0:T(8,128)(2,1)} %param.13, f32[128,1024]{1,0:T(8,128)S(1)} %fusion.9, bf16[128,4096]{1,0:T(8,128)(2,1)S(1)} %bitcast.41, bf16[1,4096,1024]{2,1,0:T(8,128)(2,1)} %param.12), kind=kOutput, calls=%fused_computation.6 | convolution fusion | flops 2149187584 | bytes 19398656 | tf_op jit(solution)/shard_map/dot_general | solution.py:41
  72.7 0.0 reduce-scatter.2.cloned.1.call-update
  72.8 26.0 %reduce-scatter.2.cloned.1.call-done = bf16[128,1024]{1,0:T(8,128)(2,1)} async-done(((bf16[128,4096]{1,0:T(8,128)(2,1)}), bf16[128,1024]{1,0:T(8,128)(2,1)}) %reduce-scatter.2.cloned.1.call-update) | async-done | bytes 262160 | tf_op jit(solution)/shard_map/reduce_scatter | solution.py:45
  98.8 4.6 %all-to-all-start.1 = ((bf16[8,16,1024]{2,1,0:T(8,128)(2,1)}), bf16[8,16,1024]{2,1,0:T(8,128)(2,1)S(1)}, u32[]{:S(2)}, u32[]{:S(2)}) async-start(bf16[8,16,1024]{2,1,0:T(8,128)(2,1)} %bitcast.47), calls=%async_computation.2 | async-start | bytes 524288 | tf_op jit(solution)/shard_map/all_to_all | solution.py:49
  103.4 0.1 select_reduce_fusion
  103.5 9.6 %all-to-all-done.1 = bf16[8,16,1024]{2,1,0:T(8,128)(2,1)S(1)} async-done(((bf16[8,16,1024]{2,1,0:T(8,128)(2,1)}), bf16[8,16,1024]{2,1,0:T(8,128)(2,1)S(1)}, u32[]{:S(2)}, u32[]{:S(2)}) %all-to-all-start.1) | async-done | bytes 262176 | tf_op jit(solution)/shard_map/all_to_all | solution.py:49
  113.1 0.8 convolution_convert_fusion.1
  (4 shorter events, 0.0 us)
Async XLA Ops:
  6.5 92.2 %reduce-scatter.2.cloned.1.call-start = ((), (), s32[]{:S(2)}) async-start(), calls=%async_computation.3 | async-start | bytes 1310720 | tf_op jit(solution)/shard_map/reduce_scatter | solution.py:45
  63.4 40.0 %copy-start = (f32[16,4]{0,1:T(4,128)S(1)}, f32[16,4]{0,1:T(4,128)}, u32[]{:S(2)}) copy-start(f32[16,4]{0,1:T(4,128)} %param.10) | copy-start | bytes 772
  98.8 14.3 %all-to-all-start.1 = ((bf16[8,16,1024]{2,1,0:T(8,128)(2,1)}), bf16[8,16,1024]{2,1,0:T(8,128)(2,1)S(1)}, u32[]{:S(2)}, u32[]{:S(2)}) async-start(bf16[8,16,1024]{2,1,0:T(8,128)(2,1)} %bitcast.47), calls=%async_computation.2 | async-start | bytes 524288 | tf_op jit(solution)/shard_map/all_to_all | solution.py:49
Sparse Core Ops, SparseCore 0:
  72.9 25.8 reduce-scatter.1
